TPU v7x, 32 devices: a whole 2x2x4 slice. The times are simulated.
32 devices in a mesh: sp: 8 (over z, y), tp: 4 (over x, core).
Axes of the slice: x: 2, y: 2, z: 4, core: 2. Of those that a mesh axis runs over, the one named last changes fastest.
Arguments:
- query_proj: bfloat16 [2048, 2048], P('sp', 'tp'), may hold values from -240 to 240
- key_projection: bfloat16 [2048, 512], P('sp', 'tp'), may hold values from -6 to 6
- value_projection: bfloat16 [2048, 512], P('sp', 'tp'), may hold values from -6 to 6
- sink_logit: float32 [32], P('tp'), may hold values from 1 to 6
- residual: bfloat16 [2048, 2048], P('sp'), may hold values from -3 to 3
- w_out: bfloat16 [2048, 2048], P('tp'), may hold values from -1 to 1
- norm_gain: float32 [2048], replicated, may hold values from 0.1 to 1.9
- routes: int32 [2048, 2], P('sp'), may hold values from 0 to 7, all different within a row; in each aligned block of 256 rows (0 to 255, 256 to 511, ...) at most 128 rows name the same one
- route_weights: float32 [2048, 2], P('sp'), may hold values from 0.1 to 1
- w_gate: bfloat16 [8, 2048, 2560], P('sp', None, 'tp'), may hold values from -0.125 to 0.125
- w_up: bfloat16 [8, 2048, 2560], P('sp', None, 'tp'), may hold values from -0.125 to 0.125
- w_down: bfloat16 [8, 2560, 2048], P('sp', 'tp'), may hold values from -0.125 to 0.125
Outputs:
- layer_out: bfloat16 [2048, 2048], P('sp', 'tp')
Inputs may be any that keep to these rules, and one draw needn't show every extreme that they name: `routes`: within the rows of one index of sp (aligned blocks of 256 tokens), no expert is named more than 128 times, and in some block one expert is named exactly 128 times. The two experts of a token differ.
All inputs are finite; a program needn't handle non-finite values.
Results may differ from a plain program's by a relative error of at most 0.015.
Values may be sent and summed in bfloat16 or wider, within the bound.
A program may use at most 64 MiB of HBM per device.

v0:
```python
import jax
import jax.numpy as jnp
from jax import lax
from jax.sharding import PartitionSpec as P

HEAD_SIZE = 64
WINDOW = 128
GRID_W = 64
ROPE_BASE = 10000.0
NORM_EPS = 1e-06


def padded(cells, sides, width):
    for axis, dim in sides:
        count = lax.axis_size(axis)
        ends = count - 1
        head = lax.slice_in_dim(cells, 0, width, axis=dim)
        tail = lax.slice_in_dim(cells, cells.shape[dim] - width, cells.shape[dim], axis=dim)
        cells = jnp.concatenate(
            [
                lax.ppermute(tail, axis, [(i, (i + 1) % count) for i in range(ends)]),
                cells,
                lax.ppermute(head, axis, [((i + 1) % count, i) for i in range(ends)]),
            ],
            axis=dim,
        )
    return cells


def rotate_pair(values_half, angles):
    first_half, second = jnp.split(values_half, 2, axis=-1)
    cosine = jnp.cos(angles)[:, None, :]
    sine_part = jnp.sin(angles)[:, None, :]
    return jnp.concatenate(
        [first_half * cosine - second * sine_part, second * cosine + first_half * sine_part],
        axis=-1,
    )


def axial_rotation(heads_in, token_positions):
    half_dim = HEAD_SIZE // 2
    inverse = ROPE_BASE ** (-jnp.arange(0, half_dim, 2, dtype=jnp.float32) / half_dim)
    row_angles = (token_positions // GRID_W).astype(jnp.float32)[:, None] * inverse
    col_angles = (token_positions % GRID_W).astype(jnp.float32)[:, None] * inverse
    as_float = heads_in.astype(jnp.float32)
    return jnp.concatenate(
        [
            rotate_pair(as_float[..., :half_dim], row_angles),
            rotate_pair(as_float[..., half_dim:], col_angles),
        ],
        axis=-1,
    )


def attend_block(query_rows, key_rows, value_rows, sink_logit, query_pos, key_pos, total_rows):
    kv_heads = key_rows.shape[1]
    groups = query_rows.shape[1] // kv_heads
    grouped = query_rows.reshape(query_rows.shape[0], kv_heads, groups, HEAD_SIZE)
    scores = jnp.einsum(
        "qkgd,jkd->kgqj", grouped, key_rows, preferred_element_type=jnp.float32
    ) * HEAD_SIZE ** (-0.5)
    in_window = (
        (jnp.abs(key_pos[None, :] - query_pos[:, None]) <= WINDOW)
        & (key_pos[None, :] >= 0)
        & (key_pos[None, :] < total_rows)
    )
    scores = jnp.where(in_window[None, None], scores, -jnp.inf)
    sink_col = sink_logit.reshape(kv_heads, groups, 1, 1)
    largest = jnp.maximum(jnp.max(scores, axis=-1, keepdims=True), sink_col)
    exp_scores = jnp.exp(scores - largest)
    denominator = jnp.sum(exp_scores, axis=-1, keepdims=True) + jnp.exp(sink_col - largest)
    weights_bf = (exp_scores / denominator).astype(jnp.bfloat16)
    mixed_heads = jnp.einsum(
        "kgqj,jkd->qkgd", weights_bf, value_rows, preferred_element_type=jnp.float32
    )
    return mixed_heads.astype(jnp.bfloat16).reshape(query_rows.shape[0], -1)


def local(
    query_proj,
    key_projection,
    value_projection,
    sink_logit,
    residual,
    w_out,
    norm_gain,
    routes,
    route_weights,
    w_gate,
    w_up,
    w_down,
):
    tok_rows = query_proj.shape[0]
    seq_devices = lax.axis_size("sp")
    total_rows = tok_rows * seq_devices
    offset = lax.axis_index("sp") * tok_rows
    kv_width = key_projection.shape[1]
    joined = jnp.concatenate([key_projection, value_projection], axis=1)
    widened = padded(joined, (("sp", 0),), WINDOW)
    query_pos = offset + jnp.arange(tok_rows, dtype=jnp.int32)
    key_pos = offset - WINDOW + jnp.arange(tok_rows + 2 * WINDOW, dtype=jnp.int32)
    rot_q = axial_rotation(query_proj.reshape(tok_rows, -1, HEAD_SIZE), query_pos).astype(
        jnp.bfloat16
    )
    rotated_keys = axial_rotation(
        widened[:, :kv_width].reshape(-1, kv_width // HEAD_SIZE, HEAD_SIZE), key_pos
    ).astype(jnp.bfloat16)
    value_head_rows = widened[:, kv_width:].reshape(-1, kv_width // HEAD_SIZE, HEAD_SIZE)
    attended = attend_block(
        rot_q, rotated_keys, value_head_rows, sink_logit, query_pos, key_pos, total_rows
    )
    partial_value = jnp.dot(attended, w_out, preferred_element_type=jnp.float32)
    width = partial_value.shape[1]
    col_blocks = lax.axis_size("tp")
    col_width = width // col_blocks
    col_start = lax.axis_index("tp") * col_width
    summed = lax.psum(partial_value.astype(jnp.bfloat16), "tp").astype(jnp.float32)
    stream = (residual.astype(jnp.float32) + summed).astype(jnp.bfloat16)
    as_float = stream.astype(jnp.float32)
    normed = (
        as_float
        * lax.rsqrt(jnp.mean(as_float * as_float, axis=-1, keepdims=True) + NORM_EPS)
        * norm_gain
    ).astype(jnp.bfloat16)
    stream_cols = lax.dynamic_slice_in_dim(stream, col_start, col_width, 1)
    top_count = routes.shape[1]
    experts = w_gate.shape[0] * seq_devices
    capacity = 2 * top_count * tok_rows // experts
    flat_routes = routes.reshape(-1)
    onehot = (flat_routes[:, None] == jnp.arange(experts, dtype=jnp.int32)[None, :]).astype(
        jnp.int32
    )
    slot_number = jnp.sum(jnp.cumsum(onehot, axis=0) * onehot, axis=1) - 1
    destination = flat_routes * capacity + slot_number
    buffer = (
        jnp.zeros((experts * capacity, width), jnp.bfloat16)
        .at[destination]
        .set(jnp.repeat(normed, top_count, axis=0))
        .reshape(experts, capacity, width)
    )
    quarter = capacity // col_blocks
    own_slots = lax.dynamic_slice_in_dim(buffer, lax.axis_index("tp") * quarter, quarter, 1)
    arrived = lax.all_to_all(own_slots, "sp", split_axis=0, concat_axis=0, tiled=True)
    joined_slots = lax.all_gather(arrived, "tp", axis=1, tiled=True)
    sources, slot_count, _ = joined_slots.shape
    expert_rows = joined_slots.reshape(-1, width)
    gate_part = jnp.dot(expert_rows, w_gate[0], preferred_element_type=jnp.float32)
    up_part = jnp.dot(expert_rows, w_up[0], preferred_element_type=jnp.float32)
    hidden = (jax.nn.silu(gate_part) * up_part).astype(jnp.bfloat16)
    partial_rows = jnp.dot(hidden, w_down[0], preferred_element_type=jnp.float32)
    col_sums = lax.psum_scatter(
        partial_rows.astype(jnp.bfloat16), "tp", scatter_dimension=1, tiled=True
    )
    returned = lax.all_to_all(
        col_sums.reshape(sources, slot_count, col_width),
        "sp",
        split_axis=0,
        concat_axis=0,
        tiled=True,
    )
    picked = (
        returned.reshape(-1, col_width)[destination]
        .astype(jnp.float32)
        .reshape(tok_rows, top_count, col_width)
    )
    mixture = jnp.sum(picked * route_weights[:, :, None], axis=1)
    return (stream_cols.astype(jnp.float32) + mixture).astype(jnp.bfloat16)


def solution(mesh):
    return jax.shard_map(
        local,
        mesh=mesh,
        in_specs=(
            P("sp", "tp"),
            P("sp", "tp"),
            P("sp", "tp"),
            P("tp"),
            P("sp", None),
            P("tp", None),
            P(),
            P("sp", None),
            P("sp", None),
            P("sp", None, "tp"),
            P("sp", None, "tp"),
            P("sp", "tp", None),
        ),
        out_specs=P("sp", "tp"),
        check_vma=False,
    )
```

profile of v0, /device:TPU:0, one launch (start us, length us, event | category | flops | bytes accessed | tf_op | source)
XLA Modules:
  0.0 277.2 jit_solution(1034085529072347477)
XLA Ops:
  9.1 5.5 %collective-permute-start = (bf16[128,256]{1,0:T(8,128)(2,1)}, bf16[128,256]{1,0:T(8,128)(2,1)}, u32[]{:S(2)}, u32[]{:S(2)}) collective-permute-start(bf16[128,256]{1,0:T(8,128)(2,1)} %get-tuple-element.21), channel_id=1, source_target_pairs={{0,4},{4,8},{8,12},{12,16},{16,20},{20,24},{24,28},{1,5},{5,9},{9,... | collective-permute-start | bytes 196616 | tf_op jit(solution)/shard_map/ppermute | solution.py:21
  14.6 1.3 collective-permute-start.1
  24.1 1.5 multiply_cosine_fusion.1
  33.7 1.7 fusion.1
  35.5 1.8 copy-done.2
  38.4 3.5 %fusion.15 = bf16[2,64,4,256]{3,1,2,0:T(8,128)(2,1)S(1)} fusion(bf16[512,2,64,1]{0,2,3,1:T(8,128)(2,1)S(1)} %bitcast.68, f32[2,512,256,4]{2,1,3,0:T(8,128)} %copy-done.2, f32[2,4,256]{2,1,0:T(4,128)S(1)} %exponential_add_fusion, f32[2,4,256]{2,1,0:T(4,128)S(1)} %broadcast_maximum_fusion, pred[256,512]{0,1:T(8,128)(4,1)S(1)} %fusion.19), kind=kOutput, calls=%fused_computation.24 | convolution fusion | flops 139591680 | bytes 4734976 | tf_op jit(solution)/shard_map/kgqj,jkd->qkgd/dot_general | solution.py:73
  42.0 1.8 convolution_convert_fusion.1
  44.2 38.5 %all-reduce.2.cloned.1.call-done = bf16[256,2048]{1,0:T(8,128)(2,1)} async-done(((bf16[256,2048]{1,0:T(8,128)(2,1)}), bf16[256,2048]{1,0:T(8,128)(2,1)}) %all-reduce.2.cloned.1.call-update) | async-done | bytes 1048592 | tf_op jit(solution)/shard_map/psum | solution.py:117
  82.7 2.0 fusion.7
  86.0 2.6 broadcast_in_dim.15
  88.6 4.1 %reshape.478 = bf16[512,2048]{1,0:T(8,128)(2,1)} reshape(bf16[256,2,2048]{2,1,0:T(2,128)(2,1)} %broadcast_in_dim.15) | data formatting | bytes 4194304 | tf_op jit(solution)/shard_map/reshape | solution.py:138
  92.7 7.2 %scatter_custom_fusion = bf16[1024,2048]{1,0:T(8,128)(2,1)} fusion(s32[512]{0:T(512)S(1)} %bitcast.73, bf16[512,2048]{1,0:T(8,128)(2,1)} %reshape.478, bf16[]{:T(256)} %constant.97.clone.1), kind=kCustom, calls=%fused_computation.20 | custom fusion | bytes 4194816 | tf_op jit(solution)/shard_map/scatter | solution.py:138
  99.9 1.3 constant_dynamic-slice_fusion
  101.2 30.7 %all_to_all.10 = bf16[8,32,2048]{2,1,0:T(8,128)(2,1)} all-to-all(bf16[8,32,2048]{2,1,0:T(8,128)(2,1)S(1)} %constant_dynamic-slice_fusion), channel_id=1, replica_groups=mesh['sp'=8,'tp'=4] {'sp'}, dimensions={0} | all-to-all | bytes 2097152 | tf_op jit(solution)/shard_map/all_to_all | solution.py:143
  132.2 33.2 %all-gather.2.cloned.1.call-done = bf16[8,128,2048]{2,1,0:T(8,128)(2,1)} async-done(((bf16[8,32,2048]{2,1,0:T(8,128)(2,1)}), bf16[8,128,2048]{2,1,0:T(8,128)(2,1)}) %all-gather.2.cloned.1.call-update) | async-done | bytes 4194320 | tf_op jit(solution)/shard_map/all_gather | solution.py:144
  165.4 8.0 %fusion.3 = f32[1024,640]{1,0:T(8,128)} fusion(bf16[1024,2048]{1,0:T(8,128)(2,1)} %bitcast.76, bf16[1,2048,640]{2,1,0:T(8,128)(2,1)} %param.22), kind=kOutput, calls=%fused_computation.11 | convolution fusion | flops 2684354560 | bytes 9437184 | tf_op jit(solution)/shard_map/dot_general | solution.py:148
  173.4 12.1 %convolution_convert_fusion = bf16[1024,2048]{1,0:T(8,128)(2,1)} fusion(bf16[1,640,2048]{2,1,0:T(8,128)(2,1)S(1)} %copy-done, f32[1024,640]{1,0:T(8,128)} %fusion.3, bf16[1024,2048]{1,0:T(8,128)(2,1)} %bitcast.77, bf16[1,2048,640]{2,1,0:T(8,128)(2,1)} %param.21), kind=kOutput, calls=%fused_computation.5 | convolution fusion | flops 5374738432 | bytes 16252928 | tf_op jit(solution)/shard_map/dot_general | solution.py:150
  185.5 44.6 %reduce-scatter.2.cloned.1.call-done = bf16[1024,512]{1,0:T(8,128)(2,1)} async-done(((bf16[1024,2048]{1,0:T(8,128)(2,1)}), bf16[1024,512]{1,0:T(8,128)(2,1)}) %reduce-scatter.2.cloned.1.call-update) | async-done | bytes 1048592 | tf_op jit(solution)/shard_map/reduce_scatter | solution.py:151
  230.1 5.5 %all-to-all-start.1 = ((bf16[8,128,512]{2,1,0:T(8,128)(2,1)}), bf16[8,128,512]{2,1,0:T(8,128)(2,1)}, u32[]{:S(2)}, u32[]{:S(2)}) async-start(bf16[8,128,512]{2,1,0:T(8,128)(2,1)} %bitcast.65), calls=%async_computation.2 | async-start | bytes 2097152 | tf_op jit(solution)/shard_map/all_to_all | solution.py:154
  235.8 25.6 %all-to-all-done.1 = bf16[8,128,512]{2,1,0:T(8,128)(2,1)} async-done(((bf16[8,128,512]{2,1,0:T(8,128)(2,1)}), bf16[8,128,512]{2,1,0:T(8,128)(2,1)}, u32[]{:S(2)}, u32[]{:S(2)}) %all-to-all-start.1) | async-done | bytes 1048608 | tf_op jit(solution)/shard_map/all_to_all | solution.py:154
  261.4 3.3 %gather_fusion = bf16[512,512]{1,0:T(8,128)(2,1)S(1)} fusion(bf16[1024,512]{1,0:T(8,128)(2,1)} %bitcast.25, s32[1024]{0:T(1024)S(1)} %pad_clamp_fusion), kind=kCustom, calls=%fused_computation | custom fusion | bytes 1050624 | tf_op jit(solution)/shard_map/gather | solution.py:162
  264.7 1.6 reshape.465
  266.3 2.6 multiply_reduce_fusion
  268.9 1.7 add_convert_fusion.1
  (68 shorter events, 21.9 us)
Async XLA Ops:
  6.5 166.9 %copy-start = (bf16[1,640,2048]{2,1,0:T(8,128)(2,1)S(1)}, bf16[1,640,2048]{2,1,0:T(8,128)(2,1)}, u32[]{:S(2)}) copy-start(bf16[1,640,2048]{2,1,0:T(8,128)(2,1)} %param.23) | copy-start | bytes 7864324
  6.5 76.1 %all-reduce.2.cloned.1.call-start = ((), (), s32[]{:S(2)}) async-start(), calls=%async_computation.3 | async-start | bytes 2097152 | tf_op jit(solution)/shard_map/psum | solution.py:117
  9.1 22.7 %collective-permute-start = (bf16[128,256]{1,0:T(8,128)(2,1)}, bf16[128,256]{1,0:T(8,128)(2,1)}, u32[]{:S(2)}, u32[]{:S(2)}) collective-permute-start(bf16[128,256]{1,0:T(8,128)(2,1)} %get-tuple-element.21), channel_id=1, source_target_pairs={{0,4},{4,8},{8,12},{12,16},{16,20},{20,24},{24,28},{1,5},{5,9},{9,... | collective-permute-start | bytes 196616 | tf_op jit(solution)/shard_map/ppermute | solution.py:21
  14.6 17.2 %collective-permute-start.1 = (bf16[128,256]{1,0:T(8,128)(2,1)}, bf16[128,256]{1,0:T(8,128)(2,1)}, u32[]{:S(2)}, u32[]{:S(2)}) collective-permute-start(bf16[128,256]{1,0:T(8,128)(2,1)} %get-tuple-element.22), channel_id=1, source_target_pairs={{4,0},{8,4},{12,8},{16,12},{20,16},{24,20},{28,24},{5,1},{9,5},{13... | collective-permute-start | bytes 196616 | tf_op jit(solution)/shard_map/ppermute | solution.py:23
  33.6 1.8 copy-start.8
  35.4 1.9 copy-start.2
  38.4 3.6 %copy-start.3 = (bf16[512,2048]{1,0:T(8,128)(2,1)S(1)}, bf16[512,2048]{1,0:T(8,128)(2,1)}, u32[]{:S(2)}) copy-start(bf16[512,2048]{1,0:T(8,128)(2,1)} %param.17) | copy-start | bytes 6291460
  42.0 2.0 copy-start.6
  42.0 2.1 copy-start.7
  42.0 2.1 copy-start.5
  43.8 41.9 %copy-start.4 = (f32[2048]{0:T(1024)S(1)}, f32[2048]{0:T(1024)}, u32[]{:S(2)}) copy-start(f32[2048]{0:T(1024)} %param.18) | copy-start | bytes 24580
  43.8 121.6 %all-gather.2.cloned.1.call-start = ((), (), s32[]{:S(2)}) async-start(), calls=%async_computation.4 | async-start | bytes 5242880 | tf_op jit(solution)/shard_map/all_gather | solution.py:144
  84.7 1.0 copy-start.1
  131.9 98.2 %reduce-scatter.2.cloned.1.call-start = ((), (), s32[]{:S(2)}) async-start(), calls=%async_computation.5 | async-start | bytes 5242880 | tf_op jit(solution)/shard_map/reduce_scatter | solution.py:151
  185.5 50.1 %copy-start.9 = (f32[256,2]{0,1:T(2,128)S(1)}, f32[256,2]{0,1:T(2,128)}, u32[]{:S(2)}) copy-start(f32[256,2]{0,1:T(2,128)} %param.20) | copy-start | bytes 6148
  230.1 31.3 %all-to-all-start.1 = ((bf16[8,128,512]{2,1,0:T(8,128)(2,1)}), bf16[8,128,512]{2,1,0:T(8,128)(2,1)}, u32[]{:S(2)}, u32[]{:S(2)}) async-start(bf16[8,128,512]{2,1,0:T(8,128)(2,1)} %bitcast.65), calls=%async_computation.2 | async-start | bytes 2097152 | tf_op jit(solution)/shard_map/all_to_all | solution.py:154
Sparse Core Ops, SparseCore 0:
  43.9 38.7 all-reduce.1
  132.0 33.3 all-gather.1
  185.6 44.4 reduce-scatter.1
where the time goes:
time: 278 us; the launch traced here: 277 us
  waiting for transfers between devices  142 us (51%)
  local copies, waits for them, and re-layouts  32.3 us (12%)
  blocking collectives  30.7 us (11%)
  matrix products  27.1 us (10%)
  other arithmetic  19 us (7%)
  between operations  13.4 us (5%)
  starting transfers between devices  12.8 us (5%)
    reduce_scatter x1, waiting for transfers between devices, local(): lax.psum_scatter(partial_rows.astype(jnp.bfloat16), 'tp', scatter_dimensi...  44.6 us
    psum x1, waiting for transfers between devices, local(): lax.psum(partial_value.astype(jnp.bfloat16), 'tp').astype(jnp.float32)  38.5 us
    all_gather x1, waiting for transfers between devices, local(): joined_slots = lax.all_gather(arrived, 'tp', axis=1, tiled=True)  33.2 us
    all_to_all x1, blocking collectives, local(): lax.all_to_all(own_slots, 'sp', split_axis=0, concat_axis=0, tiled=True)  30.7 us
    all_to_all x1, waiting for transfers between devices, local(): lax.all_to_all(col_sums.reshape(sources, slot_count, col_width), 'sp', sp...  25.6 us
    dot_general x1, matrix products, local(): jnp.dot(hidden, w_down[0], preferred_element_type=jnp.float32)  12.1 us
    dot_general x1, matrix products, local(): up_part = jnp.dot(expert_rows, w_up[0], preferred_element_type=jnp.float32)  8 us
    scatter x1, local copies, waits for them, and re-layouts, local(): buffer = jnp.zeros((experts * capacity, width), jnp.bfloat16).at[destinat...  7.21 us
  transfers between devices with their start and end apart: 6, of which 4 were waited for; matrix products, arithmetic and copies ran while one was open for 6% of the time, Pallas kernels for 0%

commit v1 on v0

--- a/solution.py
+++ b/solution.py
@@ -8,6 +8,11 @@
 GRID_W = 64
 ROPE_BASE = 10000.0
 NORM_EPS = 1e-06
+
+
+def gather_and_add(x, name):
+    blocks = lax.all_gather(x, name)
+    return jnp.sum(blocks, axis=0)
 
 
 def padded(cells, sides, width):
@@ -114,7 +119,7 @@
     col_blocks = lax.axis_size("tp")
     col_width = width // col_blocks
     col_start = lax.axis_index("tp") * col_width
-    summed = lax.psum(partial_value.astype(jnp.bfloat16), "tp").astype(jnp.float32)
+    summed = gather_and_add(partial_value.astype(jnp.bfloat16), "tp").astype(jnp.float32)
     stream = (residual.astype(jnp.float32) + summed).astype(jnp.bfloat16)
     as_float = stream.astype(jnp.float32)
     normed = (

time: 278 us -> 265 us (0.953)
  waiting for transfers between devices: 142 us -> 137 us
  local copies, waits for them, and re-layouts: 32.3 us -> 28.1 us
  other arithmetic: 19 us -> 15 us
    psum x1 -> x0, waiting for transfers between devices: 38.5 us -> none  [local(): lax.psum(partial_value.astype(jnp.bfloat16), 'tp').astype(jnp.float32)]
    all_gather x0 -> x1, waiting for transfers between devices: none -> 33.2 us  [gather_and_add(): blocks = lax.all_gather(x, name)]
    reduce_sum x0 -> x1, other arithmetic: none -> 4.25 us  [gather_and_add(): return jnp.sum(blocks, axis=0)]
    unnamed x24 -> x18, local copies, waits for them, and re-layouts: 5.85 us -> 5.18 us
  transfers between devices with their start and end apart: 6 -> 6, of which waited for: 4 -> 5; matrix products, arithmetic and copies ran while one was open for 6% -> 2% of each run, Pallas kernels for 0% -> 0%
where the time goes in v1:
time: 265 us
  waiting for transfers between devices  137 us (52%)
  blocking collectives  31.5 us (12%)
  local copies, waits for them, and re-layouts  28.1 us (11%)
  matrix products  27.1 us (10%)
  other arithmetic  15 us (6%)
  between operations  13.4 us (5%)
  starting transfers between devices  12.2 us (5%)
    reduce_scatter x1, waiting for transfers between devices, local(): lax.psum_scatter(partial_rows.astype(jnp.bfloat16), 'tp', scatter_dimensi...  44.6 us
    all_gather x1, waiting for transfers between devices, gather_and_add(): blocks = lax.all_gather(x, name)  33.2 us
    all_gather x1, waiting for transfers between devices, local(): joined_slots = lax.all_gather(arrived, 'tp', axis=1, tiled=True)  32.5 us
    all_to_all x1, blocking collectives, local(): lax.all_to_all(own_slots, 'sp', split_axis=0, concat_axis=0, tiled=True)  31.5 us
    all_to_all x1, waiting for transfers between devices, local(): lax.all_to_all(col_sums.reshape(sources, slot_count, col_width), 'sp', sp...  25.6 us
    dot_general x1, matrix products, local(): jnp.dot(hidden, w_down[0], preferred_element_type=jnp.float32)  12.1 us
    dot_general x1, matrix products, local(): up_part = jnp.dot(expert_rows, w_up[0], preferred_element_type=jnp.float32)  8 us
    scatter x1, local copies, waits for them, and re-layouts, local(): buffer = jnp.zeros((experts * capacity, width), jnp.bfloat16).at[destinat...  7.21 us
  transfers between devices with their start and end apart: 6, of which 5 were waited for; matrix products, arithmetic and copies ran while one was open for 2% of the time, Pallas kernels for 0%

profile of v1, /device:TPU:0, one launch (start us, length us, event | category | flops | bytes accessed | tf_op | source)
XLA Modules:
  0.0 264.5 jit_solution(3567403814526736775)
XLA Ops:
  8.4 4.9 %collective-permute-start = (bf16[128,256]{1,0:T(8,128)(2,1)S(1)}, bf16[128,256]{1,0:T(8,128)(2,1)S(1)}, u32[]{:S(2)}, u32[]{:S(2)}) collective-permute-start(bf16[128,256]{1,0:T(8,128)(2,1)S(1)} %get-tuple-element.21), channel_id=1, source_target_pairs={{0,4},{4,8},{8,12},{12,16},{16,20},{20,24},{24,28},{1,5},{5,9},{9,... | collective-permute-start | bytes 196616 | tf_op jit(solution)/shard_map/ppermute | solution.py:26
  18.2 1.3 collective-permute-done.1
  19.7 1.7 fusion.1
  21.6 1.8 copy-done.2
  24.5 3.5 %fusion.15 = bf16[2,64,4,256]{3,1,2,0:T(8,128)(2,1)S(1)} fusion(bf16[512,2,64,1]{0,2,3,1:T(8,128)(2,1)S(1)} %bitcast.70, f32[2,512,256,4]{2,1,3,0:T(8,128)} %copy-done.2, f32[2,4,256]{2,1,0:T(4,128)S(1)} %exponential_add_fusion, f32[2,4,256]{2,1,0:T(4,128)S(1)} %broadcast_maximum_fusion, pred[256,512]{0,1:T(8,128)(4,1)S(1)} %fusion.19), kind=kOutput, calls=%fused_computation.24 | convolution fusion | flops 139591680 | bytes 4734976 | tf_op jit(solution)/shard_map/kgqj,jkd->qkgd/dot_general | solution.py:78
  28.1 1.7 convolution_convert_fusion.1
  32.3 33.2 %all-gather.6.cloned.1.call-done = bf16[1024,2048]{1,0:T(8,128)(2,1)} async-done(((bf16[256,2048]{1,0:T(8,128)(2,1)}), bf16[1024,2048]{1,0:T(8,128)(2,1)}) %all-gather.6.cloned.1.call-update) | async-done | bytes 4194320 | tf_op jit(solution)/shard_map/all_gather | solution.py:14
  65.6 4.3 %reduce_sum.49 = bf16[256,2048]{1,0:T(8,128)(2,1)} reduce(bf16[4,256,2048]{2,1,0:T(8,128)(2,1)} %bitcast.65, bf16[]{:T(256)} %constant.96.clone.1), dimensions={0}, to_apply=%region_2.3 | reduce | flops 1572864 | bytes 5242882 | tf_op jit(solution)/shard_map/reduce_sum | solution.py:15
  69.8 2.1 fusion.7
  73.2 2.6 broadcast_in_dim.15
  75.8 4.1 %reshape.478 = bf16[512,2048]{1,0:T(8,128)(2,1)} reshape(bf16[256,2,2048]{2,1,0:T(2,128)(2,1)} %broadcast_in_dim.15) | data formatting | bytes 4194304 | tf_op jit(solution)/shard_map/reshape | solution.py:143
  79.9 7.2 %scatter_custom_fusion = bf16[1024,2048]{1,0:T(8,128)(2,1)} fusion(s32[512]{0:T(512)S(1)} %bitcast.75, bf16[512,2048]{1,0:T(8,128)(2,1)} %reshape.478, bf16[]{:T(256)} %constant.96.clone.1), kind=kCustom, calls=%fused_computation.20 | custom fusion | bytes 4194816 | tf_op jit(solution)/shard_map/scatter | solution.py:143
  87.1 1.3 constant_dynamic-slice_fusion
  88.4 31.5 %all_to_all.10 = bf16[8,32,2048]{2,1,0:T(8,128)(2,1)} all-to-all(bf16[8,32,2048]{2,1,0:T(8,128)(2,1)S(1)} %constant_dynamic-slice_fusion), channel_id=1, replica_groups=mesh['sp'=8,'tp'=4] {'sp'}, dimensions={0} | all-to-all | bytes 2097152 | tf_op jit(solution)/shard_map/all_to_all | solution.py:148
  120.3 32.5 %all-gather.4.cloned.1.call-done = bf16[8,128,2048]{2,1,0:T(8,128)(2,1)} async-done(((bf16[8,32,2048]{2,1,0:T(8,128)(2,1)}), bf16[8,128,2048]{2,1,0:T(8,128)(2,1)}) %all-gather.4.cloned.1.call-update) | async-done | bytes 4194320 | tf_op jit(solution)/shard_map/all_gather | solution.py:149
  152.7 8.0 %fusion.3 = f32[1024,640]{1,0:T(8,128)} fusion(bf16[1024,2048]{1,0:T(8,128)(2,1)} %bitcast.78, bf16[1,2048,640]{2,1,0:T(8,128)(2,1)} %param.22), kind=kOutput, calls=%fused_computation.11 | convolution fusion | flops 2684354560 | bytes 9437184 | tf_op jit(solution)/shard_map/dot_general | solution.py:153
  160.7 12.1 %convolution_convert_fusion = bf16[1024,2048]{1,0:T(8,128)(2,1)} fusion(bf16[1,640,2048]{2,1,0:T(8,128)(2,1)S(1)} %copy-done, f32[1024,640]{1,0:T(8,128)} %fusion.3, bf16[1024,2048]{1,0:T(8,128)(2,1)} %bitcast.79, bf16[1,2048,640]{2,1,0:T(8,128)(2,1)} %param.21), kind=kOutput, calls=%fused_computation.5 | convolution fusion | flops 5374738432 | bytes 16252928 | tf_op jit(solution)/shard_map/dot_general | solution.py:155
  172.8 44.6 %reduce-scatter.2.cloned.1.call-done = bf16[1024,512]{1,0:T(8,128)(2,1)} async-done(((bf16[1024,2048]{1,0:T(8,128)(2,1)}), bf16[1024,512]{1,0:T(8,128)(2,1)}) %reduce-scatter.2.cloned.1.call-update) | async-done | bytes 1048592 | tf_op jit(solution)/shard_map/reduce_scatter | solution.py:156
  217.4 5.5 %all-to-all-start.1 = ((bf16[8,128,512]{2,1,0:T(8,128)(2,1)}), bf16[8,128,512]{2,1,0:T(8,128)(2,1)}, u32[]{:S(2)}, u32[]{:S(2)}) async-start(bf16[8,128,512]{2,1,0:T(8,128)(2,1)} %bitcast.67), calls=%async_computation.2 | async-start | bytes 2097152 | tf_op jit(solution)/shard_map/all_to_all | solution.py:159
  223.1 25.6 %all-to-all-done.1 = bf16[8,128,512]{2,1,0:T(8,128)(2,1)} async-done(((bf16[8,128,512]{2,1,0:T(8,128)(2,1)}), bf16[8,128,512]{2,1,0:T(8,128)(2,1)}, u32[]{:S(2)}, u32[]{:S(2)}) %all-to-all-start.1) | async-done | bytes 1048608 | tf_op jit(solution)/shard_map/all_to_all | solution.py:159
  248.7 3.3 %gather_fusion = bf16[512,512]{1,0:T(8,128)(2,1)S(1)} fusion(bf16[1024,512]{1,0:T(8,128)(2,1)} %bitcast.26, s32[1024]{0:T(1024)S(1)} %pad_clamp_fusion), kind=kCustom, calls=%fused_computation | custom fusion | bytes 1050624 | tf_op jit(solution)/shard_map/gather | solution.py:167
  252.0 1.6 reshape.465
  253.7 2.6 multiply_reduce_fusion
  256.3 1.7 add_convert_fusion.1
  (63 shorter events, 12.2 us)
Async XLA Ops:
  6.5 154.2 %copy-start = (bf16[1,640,2048]{2,1,0:T(8,128)(2,1)S(1)}, bf16[1,640,2048]{2,1,0:T(8,128)(2,1)}, u32[]{:S(2)}) copy-start(bf16[1,640,2048]{2,1,0:T(8,128)(2,1)} %param.23) | copy-start | bytes 7864324
  6.5 59.0 %all-gather.6.cloned.1.call-start = ((), (), s32[]{:S(2)}) async-start(), calls=%async_computation.5 | async-start | bytes 5242880 | tf_op jit(solution)/shard_map/all_gather | solution.py:14
  8.4 9.7 %collective-permute-start = (bf16[128,256]{1,0:T(8,128)(2,1)S(1)}, bf16[128,256]{1,0:T(8,128)(2,1)S(1)}, u32[]{:S(2)}, u32[]{:S(2)}) collective-permute-start(bf16[128,256]{1,0:T(8,128)(2,1)S(1)} %get-tuple-element.21), channel_id=1, source_target_pairs={{0,4},{4,8},{8,12},{12,16},{16,20},{20,24},{24,28},{1,5},{5,9},{9,... | collective-permute-start | bytes 196616 | tf_op jit(solution)/shard_map/ppermute | solution.py:26
  13.3 6.2 %collective-permute-start.1 = (bf16[128,256]{1,0:T(8,128)(2,1)S(1)}, bf16[128,256]{1,0:T(8,128)(2,1)S(1)}, u32[]{:S(2)}, u32[]{:S(2)}) collective-permute-start(bf16[128,256]{1,0:T(8,128)(2,1)S(1)} %get-tuple-element.22), channel_id=1, source_target_pairs={{4,0},{8,4},{12,8},{16,12},{20,16},{24,20},{28,24},{5,1},{9,5},{13... | collective-permute-start | bytes 196616 | tf_op jit(solution)/shard_map/ppermute | solution.py:28
  21.5 1.9 copy-start.2
  24.5 3.6 %copy-start.3 = (bf16[512,2048]{1,0:T(8,128)(2,1)S(1)}, bf16[512,2048]{1,0:T(8,128)(2,1)}, u32[]{:S(2)}) copy-start(bf16[512,2048]{1,0:T(8,128)(2,1)} %param.17) | copy-start | bytes 6291460
  28.1 2.0 copy-start.5
  29.8 122.9 %all-gather.4.cloned.1.call-start = ((), (), s32[]{:S(2)}) async-start(), calls=%async_computation.3 | async-start | bytes 5242880 | tf_op jit(solution)/shard_map/all_gather | solution.py:149
  69.8 3.0 %copy-start.4 = (f32[2048]{0:T(1024)S(1)}, f32[2048]{0:T(1024)}, u32[]{:S(2)}) copy-start(f32[2048]{0:T(1024)} %param.18) | copy-start | bytes 24580
  71.9 1.0 copy-start.1
  120.0 97.4 %reduce-scatter.2.cloned.1.call-start = ((), (), s32[]{:S(2)}) async-start(), calls=%async_computation.4 | async-start | bytes 5242880 | tf_op jit(solution)/shard_map/reduce_scatter | solution.py:156
  172.8 50.1 %copy-start.6 = (f32[256,2]{0,1:T(2,128)S(1)}, f32[256,2]{0,1:T(2,128)}, u32[]{:S(2)}) copy-start(f32[256,2]{0,1:T(2,128)} %param.20) | copy-start | bytes 6148
  217.4 31.3 %all-to-all-start.1 = ((bf16[8,128,512]{2,1,0:T(8,128)(2,1)}), bf16[8,128,512]{2,1,0:T(8,128)(2,1)}, u32[]{:S(2)}, u32[]{:S(2)}) async-start(bf16[8,128,512]{2,1,0:T(8,128)(2,1)} %bitcast.67), calls=%async_computation.2 | async-start | bytes 2097152 | tf_op jit(solution)/shard_map/all_to_all | solution.py:159
Sparse Core Ops, SparseCore 0:
  29.9 35.5 all-gather.5
  120.1 32.5 all-gather.3
  173.0 44.4 reduce-scatter.1
